TPU v7x, 32 devices: a whole 2x2x4 slice. The times are simulated.
32 devices in a mesh: grp: 1, ep: 16 (over z, y, x), tp: 2 (over core).
Axes of the slice: x: 2, y: 2, z: 4, core: 2. Of those that a mesh axis runs over, the one named last changes fastest.
Arguments:
- tokens_in: bfloat16 [1024, 2048], P(('grp', 'ep')), may hold values from -6 to 6
- norm_gain: float32 [2048], replicated, may hold values from 0.1 to 1.9
- gate_proj: bfloat16 [16, 2048, 1024], P('ep', None, 'tp'), may hold values from -0.125 to 0.125
- up_proj: bfloat16 [16, 2048, 1024], P('ep', None, 'tp'), may hold values from -0.125 to 0.125
- down_proj: bfloat16 [16, 1024, 2048], P('ep', 'tp'), may hold values from -0.1875 to 0.1875
- route_ids: int32 [1024, 8], P(('grp', 'ep')), may hold values from 0 to 15, all different within a row; in each aligned block of 64 rows (0 to 63, 64 to 127, ...) at most 64 rows name the same one
- group_weight: float32 [1024, 2], P(('grp', 'ep')), may hold values from 0.05 to 1
- expert_weight: float32 [1024, 8], P(('grp', 'ep')), may hold values from 0.05 to 1
Outputs:
- expert_mix: bfloat16 [1024, 2048], P(('grp', 'ep'), 'tp')
Inputs may be any that keep to these rules, and one draw needn't show every extreme that they name: `route_ids`: each row names 8 different experts; within the rows of one index of ep no expert is named by more than 64 rows, a bound that some of them reach.
All inputs are finite; a program needn't handle non-finite values.
Results may differ from a plain program's by a relative error of at most 0.0077.
Values may be sent and summed in bfloat16 or wider, within the bound.
A program may use at most 64 MiB of HBM per device.

v0:
```python
import jax
import jax.numpy as jnp
from jax import lax
from jax.sharding import PartitionSpec as P

TOP = 8
EXP_GRP = 8
EPSILON = 1e-06


def on_device(
    tokens_in, norm_gain, gate_proj, up_proj, down_proj, route_ids, group_weight, expert_weight
):
    token_count, model_width = tokens_in.shape
    expert_count = gate_proj.shape[0] * lax.axis_size("ep")
    lane_count = lax.axis_size("tp")
    part_width = model_width // lane_count
    capacity = min(token_count, max(2, 2 * token_count * TOP // expert_count))
    slot_total = expert_count * capacity
    row_values = tokens_in.astype(jnp.float32)
    inv_scale = lax.rsqrt(jnp.mean(row_values * row_values, axis=-1, keepdims=True) + EPSILON)
    normed = (row_values * inv_scale * norm_gain).astype(jnp.bfloat16)
    route_count = token_count * TOP
    flat_ids = route_ids.reshape(route_count)
    positions = jnp.arange(route_count, dtype=jnp.int32)
    same_expert = (flat_ids[:, None] == flat_ids[None, :]) & (
        positions[None, :] < positions[:, None]
    )
    slot_rank = jnp.sum(same_expert.astype(jnp.int32), axis=1)
    slot_index = flat_ids * capacity + slot_rank
    slot_match = jnp.arange(slot_total, dtype=jnp.int32)[:, None] == slot_index[None, :]
    selector = jnp.sum(
        slot_match.reshape(slot_total, token_count, TOP).astype(jnp.int32), axis=2
    ).astype(jnp.bfloat16)
    gate_local = gate_proj[0]
    up_local = up_proj[0]
    lane_index = lax.axis_index("tp")
    own_half = lax.dynamic_slice_in_dim(normed, lane_index * part_width, part_width, 1)
    outgoing = jnp.dot(selector, own_half, preferred_element_type=jnp.float32).astype(jnp.bfloat16)
    arrived = lax.all_to_all(
        outgoing.reshape(expert_count, capacity, part_width),
        "ep",
        split_axis=0,
        concat_axis=0,
        tiled=True,
    )
    arrived = arrived.reshape(slot_total, part_width)
    column_piece = lax.all_gather(arrived, "tp", axis=1, tiled=True)
    gate_acts = jnp.dot(column_piece, gate_local, preferred_element_type=jnp.float32)
    up_acts = jnp.dot(column_piece, up_local, preferred_element_type=jnp.float32)
    hidden = (jax.nn.silu(gate_acts) * up_acts).astype(jnp.bfloat16)
    partial_rows = jnp.dot(hidden, down_proj[0], preferred_element_type=jnp.float32)
    summed = lax.psum_scatter(
        partial_rows.reshape(expert_count, capacity, model_width).astype(jnp.bfloat16),
        "tp",
        scatter_dimension=2,
        tiled=True,
    )
    returned = lax.all_to_all(summed, "ep", split_axis=0, concat_axis=0, tiled=True).reshape(
        slot_total, part_width
    )
    picked = returned[slot_index].astype(jnp.float32).reshape(token_count, TOP, part_width)
    group_ids = route_ids // EXP_GRP
    group_count = group_weight.shape[1]
    group_match = (
        group_ids[:, :, None] == jnp.arange(group_count, dtype=jnp.int32)[None, None, :]
    ).astype(jnp.float32)
    group_part = jnp.sum(group_weight[:, None, :] * group_match, axis=2)
    gate_values = group_part * expert_weight / jnp.sum(expert_weight, axis=1, keepdims=True)
    return jnp.sum(picked * gate_values[:, :, None], axis=1).astype(jnp.bfloat16)


def solution(mesh):
    in_specs = (
        P(("grp", "ep"), None),
        P(),
        P("ep", None, "tp"),
        P("ep", None, "tp"),
        P("ep", "tp", None),
        P(("grp", "ep"), None),
        P(("grp", "ep"), None),
        P(("grp", "ep"), None),
    )
    out_specs = P(("grp", "ep"), "tp")
    return jax.shard_map(
        on_device, mesh=mesh, in_specs=in_specs, out_specs=out_specs, check_vma=False
    )
```

profile of v0, /device:TPU:12, one launch (start us, length us, event | category | flops | bytes accessed | tf_op | source)
XLA Modules:
  0.0 173.9 jit_solution(4123312563667947729)
XLA Ops:
  6.5 1.1 convert_element_type.38
  7.7 1.1 multiply_reduce_fusion
  8.8 0.8 copy.18
  9.6 0.1 eq.43
  9.7 0.3 convert_reduce_fusion.1
  9.9 0.1 reduce_sum.59
  10.0 0.7 convert_reduce_fusion
  10.7 0.7 dynamic-slice
  11.4 0.8 convolution_convert_fusion.1
  12.2 54.7 %all_to_all.10 = bf16[16,64,1024]{2,1,0:T(8,128)(2,1)} all-to-all(bf16[16,64,1024]{2,1,0:T(8,128)(2,1)S(1)} %bitcast.25), channel_id=1, replica_groups=mesh['grp'=1,'ep'=16,'tp'=2] {'ep'}, dimensions={0} | all-to-all | bytes 4194304 | tf_op jit(solution)/shard_map/all_to_all | solution.py:40
  66.9 0.0 all-gather.2.cloned.1.call-update
  66.9 0.0 reduce-scatter.2.cloned.1.call-start
  67.0 13.1 %all-gather.2.cloned.1.call-done = bf16[1024,2048]{1,0:T(8,128)(2,1)} async-done(((bf16[1024,1024]{1,0:T(8,128)(2,1)}), bf16[1024,2048]{1,0:T(8,128)(2,1)}) %all-gather.2.cloned.1.call-update) | async-done | bytes 4194320 | tf_op jit(solution)/shard_map/all_gather | solution.py:48
  80.1 5.3 %fusion.2 = f32[1024,512]{1,0:T(8,128)S(1)} fusion(bf16[1024,2048]{1,0:T(8,128)(2,1)} %all-gather.2.cloned.1.call-done, bf16[1,2048,512]{2,1,0:T(8,128)(2,1)} %param.11), kind=kOutput, calls=%fused_computation.5 | convolution fusion | flops 2147483648 | bytes 8388608 | tf_op jit(solution)/shard_map/dot_general | solution.py:50
  85.4 2.6 %multiply_convert_fusion = bf16[1024,512]{1,0:T(8,128)(2,1)S(1)} fusion(f32[1024,512]{1,0:T(8,128)S(1)} %fusion.2, bf16[1024,2048]{1,0:T(8,128)(2,1)S(1)} %copy-done.4, bf16[1,2048,512]{2,1,0:T(8,128)(2,1)S(1)} %copy-done.5), kind=kOutput, calls=%fused_computation.9 | convolution fusion | flops 2150629376 | bytes 9437184 | tf_op jit(solution)/shard_map/dot_general | solution.py:49
  88.1 4.3 %convolution_convert_fusion = bf16[16,64,2048]{2,1,0:T(8,128)(2,1)} fusion(bf16[16,64,512]{2,1,0:T(8,128)(2,1)S(1)} %bitcast.28, bf16[1,512,2048]{2,1,0:T(8,128)(2,1)S(1)} %copy-done), kind=kOutput, calls=%fused_computation.1 | convolution fusion | flops 2149580800 | bytes 7340032 | tf_op jit(solution)/shard_map/dot_general | solution.py:52
  92.3 0.0 reduce-scatter.2.cloned.1.call-update
  92.4 13.3 %reduce-scatter.2.cloned.1.call-done = bf16[16,64,1024]{2,1,0:T(8,128)(2,1)} async-done(((bf16[16,64,2048]{2,1,0:T(8,128)(2,1)}), bf16[16,64,1024]{2,1,0:T(8,128)(2,1)}) %reduce-scatter.2.cloned.1.call-update) | async-done | bytes 2097168 | tf_op jit(solution)/shard_map/reduce_scatter | solution.py:53
  105.7 7.0 %all-to-all-start.1 = ((bf16[16,64,1024]{2,1,0:T(8,128)(2,1)}), bf16[16,64,1024]{2,1,0:T(8,128)(2,1)}, u32[]{:S(2)}, u32[]{:S(2)}) async-start(bf16[16,64,1024]{2,1,0:T(8,128)(2,1)} %reduce-scatter.2.cloned.1.call-done), calls=%async_computation.2 | async-start | bytes 4194304 | tf_op jit(solution)/shard_map/all_to_all | solution.py:59
  112.6 0.1 mul.78
  112.8 0.1 copy.20
  112.9 48.2 %all-to-all-done.1 = bf16[16,64,1024]{2,1,0:T(8,128)(2,1)} async-done(((bf16[16,64,1024]{2,1,0:T(8,128)(2,1)}), bf16[16,64,1024]{2,1,0:T(8,128)(2,1)}, u32[]{:S(2)}, u32[]{:S(2)}) %all-to-all-start.1) | async-done | bytes 2097184 | tf_op jit(solution)/shard_map/all_to_all | solution.py:59
  161.1 4.6 %gather_fusion = bf16[512,1024]{1,0:T(8,128)(2,1)S(1)} fusion(bf16[1024,1024]{1,0:T(8,128)(2,1)} %bitcast.7, s32[1024]{0:T(1024)S(1)} %pad_clamp_fusion), kind=kCustom, calls=%fused_computation | custom fusion | bytes 2099200 | tf_op jit(solution)/shard_map/gather | solution.py:62
  165.7 1.4 fusion
  (21 shorter events, 0.1 us)
Async XLA Ops:
  6.5 81.5 %copy-start = (bf16[1,512,2048]{2,1,0:T(8,128)(2,1)S(1)}, bf16[1,512,2048]{2,1,0:T(8,128)(2,1)}, u32[]{:S(2)}) copy-start(bf16[1,512,2048]{2,1,0:T(8,128)(2,1)} %param.12) | copy-start | bytes 6291460
  6.5 73.5 %all-gather.2.cloned.1.call-start = ((), (), s32[]{:S(2)}) async-start(), calls=%async_computation.3 | async-start | bytes 6291456 | tf_op jit(solution)/shard_map/all_gather | solution.py:48
  66.9 38.8 %reduce-scatter.2.cloned.1.call-start = ((), (), s32[]{:S(2)}) async-start(), calls=%async_computation.4 | async-start | bytes 6291456 | tf_op jit(solution)/shard_map/reduce_scatter | solution.py:53
  80.0 5.3 %copy-start.4 = (bf16[1024,2048]{1,0:T(8,128)(2,1)S(1)}, bf16[1024,2048]{1,0:T(8,128)(2,1)}, u32[]{:S(2)}) copy-start(bf16[1024,2048]{1,0:T(8,128)(2,1)} %all-gather.2.cloned.1.call-done) | copy-start | bytes 12582916
  80.1 5.3 %copy-start.5 = (bf16[1,2048,512]{2,1,0:T(8,128)(2,1)S(1)}, bf16[1,2048,512]{2,1,0:T(8,128)(2,1)}, u32[]{:S(2)}) copy-start(bf16[1,2048,512]{2,1,0:T(8,128)(2,1)} %param.10) | copy-start | bytes 6291460
  92.4 20.4 %copy-start.1 = (f32[64,8]{0,1:T(8,128)S(1)}, f32[64,8]{0,1:T(8,128)}, u32[]{:S(2)}) copy-start(f32[64,8]{0,1:T(8,128)} %param.15) | copy-start | bytes 6148
  92.4 20.4 %copy-start.2 = (s32[64,8]{0,1:T(8,128)S(1)}, s32[64,8]{0,1:T(8,128)}, u32[]{:S(2)}) copy-start(s32[64,8]{0,1:T(8,128)} %param.13) | copy-start | bytes 6148
  92.4 20.4 %copy-start.3 = (f32[64,2]{0,1:T(2,128)S(1)}, f32[64,2]{0,1:T(2,128)}, u32[]{:S(2)}) copy-start(f32[64,2]{0,1:T(2,128)} %param.14) | copy-start | bytes 1540
  105.7 55.4 %all-to-all-start.1 = ((bf16[16,64,1024]{2,1,0:T(8,128)(2,1)}), bf16[16,64,1024]{2,1,0:T(8,128)(2,1)}, u32[]{:S(2)}, u32[]{:S(2)}) async-start(bf16[16,64,1024]{2,1,0:T(8,128)(2,1)} %reduce-scatter.2.cloned.1.call-done), calls=%async_computation.2 | async-start | bytes 4194304 | tf_op jit(solution)/shard_map/all_to_all | solution.py:59
Sparse Core Ops, SparseCore 0:
  67.0 12.9 all-gather.1
  92.5 13.1 reduce-scatter.1
where the time goes:
time: 174 us
  waiting for transfers between devices  74.6 us (43%)
  blocking collectives  54.7 us (31%)
  between operations  13.6 us (8%)
  matrix products  13 us (7%)
  starting transfers between devices  7.01 us (4%)
  local copies, waits for them, and re-layouts  6.44 us (4%)
  other arithmetic  4.59 us (3%)
    all_to_all x1, blocking collectives, on_device(): lax.all_to_all(outgoing.reshape(expert_count, capacity, part_width), 'ep'...  54.7 us
    all_to_all x1, waiting for transfers between devices, on_device(): lax.all_to_all(summed, 'ep', split_axis=0, concat_axis=0, tiled=True)  48.2 us
    reduce_scatter x1, waiting for transfers between devices, on_device(): lax.psum_scatter(partial_rows.reshape(expert_count, capacity, model_width...  13.3 us
    all_gather x1, waiting for transfers between devices, on_device(): column_piece = lax.all_gather(arrived, 'tp', axis=1, tiled=True)  13.1 us
    all_to_all x1, starting transfers between devices, on_device(): lax.all_to_all(summed, 'ep', split_axis=0, concat_axis=0, tiled=True)  6.97 us
    dot_general x1, matrix products, on_device(): jnp.dot(column_piece, up_local, preferred_element_type=jnp.float32)  5.32 us
    gather x1, local copies, waits for them, and re-layouts, on_device(): returned[slot_index].astype(jnp.float32)  4.59 us
    dot_general x1, matrix products, on_device(): jnp.dot(hidden, down_proj[0], preferred_element_type=jnp.float32)  4.27 us
  transfers between devices with their start and end apart: 3, of which 3 were waited for; matrix products, arithmetic and copies ran while one was open for 0% of the time, Pallas kernels for 0%

commit v1 on v0

--- a/solution.py
+++ b/solution.py
@@ -45,7 +45,7 @@
         tiled=True,
     )
     arrived = arrived.reshape(slot_total, part_width)
-    column_piece = lax.all_gather(arrived, "tp", axis=1, tiled=True)
+    column_piece = jnp.concatenate(lax.all_gather(arrived, "tp"), axis=1)
     gate_acts = jnp.dot(column_piece, gate_local, preferred_element_type=jnp.float32)
     up_acts = jnp.dot(column_piece, up_local, preferred_element_type=jnp.float32)
     hidden = (jax.nn.silu(gate_acts) * up_acts).astype(jnp.bfloat16)

time: 174 us -> 181 us (1.040)
  local copies, waits for them, and re-layouts: 6.44 us -> 12.7 us
    all_gather x0 -> x1, local copies, waits for them, and re-layouts: none -> 6.21 us  [on_device(): column_piece = jnp.concatenate(lax.all_gather(arrived, 'tp'), axis=1)]
where the time goes in v1:
time: 181 us; the launch traced here: 180 us
  waiting for transfers between devices  74.6 us (41%)
  blocking collectives  54.7 us (30%)
  between operations  13.6 us (8%)
  matrix products  13.1 us (7%)
  local copies, waits for them, and re-layouts  12.7 us (7%)
  starting transfers between devices  7.02 us (4%)
  other arithmetic  4.58 us (3%)
    all_to_all x1, blocking collectives, on_device(): lax.all_to_all(outgoing.reshape(expert_count, capacity, part_width), 'ep'...  54.7 us
    all_to_all x1, waiting for transfers between devices, on_device(): lax.all_to_all(summed, 'ep', split_axis=0, concat_axis=0, tiled=True)  48.2 us
    reduce_scatter x1, waiting for transfers between devices, on_device(): lax.psum_scatter(partial_rows.reshape(expert_count, capacity, model_width...  13.3 us
    all_gather x1, waiting for transfers between devices, on_device(): column_piece = jnp.concatenate(lax.all_gather(arrived, 'tp'), axis=1)  13.1 us
    all_to_all x1, starting transfers between devices, on_device(): lax.all_to_all(summed, 'ep', split_axis=0, concat_axis=0, tiled=True)  6.98 us
    all_gather x1, local copies, waits for them, and re-layouts, on_device(): column_piece = jnp.concatenate(lax.all_gather(arrived, 'tp'), axis=1)  6.21 us
    dot_general x1, matrix products, on_device(): jnp.dot(column_piece, up_local, preferred_element_type=jnp.float32)  5.37 us
    gather x1, local copies, waits for them, and re-layouts, on_device(): returned[slot_index].astype(jnp.float32)  4.59 us
  transfers between devices with their start and end apart: 3, of which 3 were waited for; matrix products, arithmetic and copies ran while one was open for 0% of the time, Pallas kernels for 0%

profile of v1, /device:TPU:12, one launch (start us, length us, event | category | flops | bytes accessed | tf_op | source)
XLA Modules:
  0.0 180.2 jit_solution(4555639858698219779)
XLA Ops:
  6.5 1.1 convert_element_type.38
  7.7 1.1 multiply_reduce_fusion
  8.8 0.8 copy.31
  9.6 0.1 eq.43
  9.7 0.3 convert_reduce_fusion.1
  9.9 0.1 reduce_sum.59
  10.0 0.7 convert_reduce_fusion
  10.7 0.7 dynamic-slice
  11.4 0.8 convolution_convert_fusion.1
  12.2 54.7 %all_to_all.10 = bf16[16,64,1024]{2,1,0:T(8,128)(2,1)} all-to-all(bf16[16,64,1024]{2,1,0:T(8,128)(2,1)S(1)} %bitcast.30), channel_id=1, replica_groups=mesh['grp'=1,'ep'=16,'tp'=2] {'ep'}, dimensions={0} | all-to-all | bytes 4194304 | tf_op jit(solution)/shard_map/all_to_all | solution.py:40
  66.9 0.0 all-gather.2.cloned.1.call-update
  66.9 0.0 reduce-scatter.2.cloned.1.call-start
  67.0 13.1 %all-gather.2.cloned.1.call-done = bf16[2,1024,1024]{2,1,0:T(8,128)(2,1)} async-done(((bf16[1,1024,1024]{2,1,0:T(8,128)(2,1)}), bf16[2,1024,1024]{2,1,0:T(8,128)(2,1)}) %all-gather.2.cloned.1.call-update) | async-done | bytes 4194320 | tf_op jit(solution)/shard_map/all_gather | solution.py:48
  80.0 6.2 %copy.33 = bf16[2,1024,1024]{1,2,0:T(8,128)(2,1)} copy(bf16[2,1024,1024]{2,1,0:T(8,128)(2,1)} %all-gather.2.cloned.1.call-done) | data formatting | bytes 8388608 | tf_op jit(solution)/shard_map/all_gather | solution.py:48
  86.3 5.4 %fusion.2 = f32[1024,512]{1,0:T(8,128)S(1)} fusion(bf16[1024,2048]{0,1:T(8,128)(2,1)} %bitcast.27, bf16[1,2048,512]{2,1,0:T(8,128)(2,1)} %param.11), kind=kOutput, calls=%fused_computation.5 | convolution fusion | flops 2147483648 | bytes 8388608 | tf_op jit(solution)/shard_map/dot_general | solution.py:50
  91.6 2.7 %multiply_convert_fusion = bf16[1024,512]{1,0:T(8,128)(2,1)S(1)} fusion(f32[1024,512]{1,0:T(8,128)S(1)} %fusion.2, bf16[1024,2048]{0,1:T(8,128)(2,1)S(1)} %bitcast.28, bf16[1,2048,512]{2,1,0:T(8,128)(2,1)S(1)} %copy-done.5), kind=kOutput, calls=%fused_computation.9 | convolution fusion | flops 2150629376 | bytes 9437184 | tf_op jit(solution)/shard_map/dot_general | solution.py:49
  94.4 4.3 %convolution_convert_fusion = bf16[16,64,2048]{2,1,0:T(8,128)(2,1)} fusion(bf16[16,64,512]{2,1,0:T(8,128)(2,1)S(1)} %bitcast.33, bf16[1,512,2048]{2,1,0:T(8,128)(2,1)S(1)} %copy-done), kind=kOutput, calls=%fused_computation.1 | convolution fusion | flops 2149580800 | bytes 7340032 | tf_op jit(solution)/shard_map/dot_general | solution.py:52
  98.7 13.3 %reduce-scatter.2.cloned.1.call-done = bf16[16,64,1024]{2,1,0:T(8,128)(2,1)} async-done(((bf16[16,64,2048]{2,1,0:T(8,128)(2,1)}), bf16[16,64,1024]{2,1,0:T(8,128)(2,1)}) %reduce-scatter.2.cloned.1.call-update) | async-done | bytes 2097168 | tf_op jit(solution)/shard_map/reduce_scatter | solution.py:53
  112.0 7.0 %all-to-all-start.1 = ((bf16[16,64,1024]{2,1,0:T(8,128)(2,1)}), bf16[16,64,1024]{2,1,0:T(8,128)(2,1)}, u32[]{:S(2)}, u32[]{:S(2)}) async-start(bf16[16,64,1024]{2,1,0:T(8,128)(2,1)} %reduce-scatter.2.cloned.1.call-done), calls=%async_computation.2 | async-start | bytes 4194304 | tf_op jit(solution)/shard_map/all_to_all | solution.py:59
  119.0 0.1 mul.78
  119.1 0.1 copy.34
  119.2 48.2 %all-to-all-done.1 = bf16[16,64,1024]{2,1,0:T(8,128)(2,1)} async-done(((bf16[16,64,1024]{2,1,0:T(8,128)(2,1)}), bf16[16,64,1024]{2,1,0:T(8,128)(2,1)}, u32[]{:S(2)}, u32[]{:S(2)}) %all-to-all-start.1) | async-done | bytes 2097184 | tf_op jit(solution)/shard_map/all_to_all | solution.py:59
  167.4 4.6 %gather_fusion = bf16[512,1024]{1,0:T(8,128)(2,1)S(1)} fusion(bf16[1024,1024]{1,0:T(8,128)(2,1)} %bitcast.10, s32[1024]{0:T(1024)S(1)} %pad_clamp_fusion), kind=kCustom, calls=%fused_computation | custom fusion | bytes 2099200 | tf_op jit(solution)/shard_map/gather | solution.py:62
  172.0 1.3 fusion
  (22 shorter events, 0.1 us)
Async XLA Ops:
  6.5 87.8 %copy-start = (bf16[1,512,2048]{2,1,0:T(8,128)(2,1)S(1)}, bf16[1,512,2048]{2,1,0:T(8,128)(2,1)}, u32[]{:S(2)}) copy-start(bf16[1,512,2048]{2,1,0:T(8,128)(2,1)} %param.12) | copy-start | bytes 6291460
  6.5 73.5 %all-gather.2.cloned.1.call-start = ((), (), s32[]{:S(2)}) async-start(), calls=%async_computation.3 | async-start | bytes 6291456 | tf_op jit(solution)/shard_map/all_gather | solution.py:48
  66.9 45.1 %reduce-scatter.2.cloned.1.call-start = ((), (), s32[]{:S(2)}) async-start(), calls=%async_computation.4 | async-start | bytes 6291456 | tf_op jit(solution)/shard_map/reduce_scatter | solution.py:53
  86.3 5.4 %copy-start.1 = (bf16[2,1024,1024]{1,2,0:T(8,128)(2,1)S(1)}, bf16[2,1024,1024]{1,2,0:T(8,128)(2,1)}, u32[]{:S(2)}) copy-start(bf16[2,1024,1024]{1,2,0:T(8,128)(2,1)} %copy.33) | copy-start | bytes 12582916
  86.3 5.4 %copy-start.5 = (bf16[1,2048,512]{2,1,0:T(8,128)(2,1)S(1)}, bf16[1,2048,512]{2,1,0:T(8,128)(2,1)}, u32[]{:S(2)}) copy-start(bf16[1,2048,512]{2,1,0:T(8,128)(2,1)} %param.10) | copy-start | bytes 6291460
  98.7 20.4 %copy-start.2 = (f32[64,8]{0,1:T(8,128)S(1)}, f32[64,8]{0,1:T(8,128)}, u32[]{:S(2)}) copy-start(f32[64,8]{0,1:T(8,128)} %param.15) | copy-start | bytes 6148
  98.7 20.4 %copy-start.3 = (s32[64,8]{0,1:T(8,128)S(1)}, s32[64,8]{0,1:T(8,128)}, u32[]{:S(2)}) copy-start(s32[64,8]{0,1:T(8,128)} %param.13) | copy-start | bytes 6148
  98.7 20.4 %copy-start.4 = (f32[64,2]{0,1:T(2,128)S(1)}, f32[64,2]{0,1:T(2,128)}, u32[]{:S(2)}) copy-start(f32[64,2]{0,1:T(2,128)} %param.14) | copy-start | bytes 1540
  112.0 55.5 %all-to-all-start.1 = ((bf16[16,64,1024]{2,1,0:T(8,128)(2,1)}), bf16[16,64,1024]{2,1,0:T(8,128)(2,1)}, u32[]{:S(2)}, u32[]{:S(2)}) async-start(bf16[16,64,1024]{2,1,0:T(8,128)(2,1)} %reduce-scatter.2.cloned.1.call-done), calls=%async_computation.2 | async-start | bytes 4194304 | tf_op jit(solution)/shard_map/all_to_all | solution.py:59
Sparse Core Ops, SparseCore 0:
  67.0 12.9 all-gather.1
  98.8 13.1 reduce-scatter.1
